TPU v7x, 32 devices: a whole 2x2x4 slice. The times are simulated.
32 devices in a mesh: sp: 16 (over z, y, core), tp: 2 (over x).
Axes of the slice: x: 2, y: 2, z: 4, core: 2. Of those that a mesh axis runs over, the one named last changes fastest.
Arguments:
- queries: bfloat16 [16384, 1024], P('sp', 'tp'), may hold values from -8 to 8
- keyvals: bfloat16 [16384, 8, 128], P('sp', 'tp'), may hold values from -8 to 8
- head_sink_logit: float32 [16], P('tp'), may hold values from 2 to 7
- doc_ids: int32 [16384], P('sp'), may hold values from 0 to 7, never falling along the last dimension, each value on 1 to 4096 neighbouring positions
- stream_in: bfloat16 [16384, 2048], P(('sp', 'tp')), may hold values from -6 to 6
- out_weight: bfloat16 [1024, 2048], replicated, may hold values from -1.5 to 1.5
- first_gain: float32 [2048], replicated, may hold values from 0.1 to 1.9
- up_weight: bfloat16 [2048, 8192], P('sp', 'tp'), may hold values from -0.125 to 0.125
- down_weight: bfloat16 [8192, 2048], P('tp', 'sp'), may hold values from -0.0625 to 0.0625
- second_gain: float32 [2048], replicated, may hold values from 0.1 to 1.9
Outputs:
- layer_out: bfloat16 [16384, 2048], P(('sp', 'tp'))
Inputs may be any that keep to these rules, and one draw needn't show every extreme that they name: `doc_ids`: document numbers never fall along the sequence.
All inputs are finite; a program needn't handle non-finite values.
Results may differ from a plain program's by a relative error of at most 0.013.
Values may be sent and summed in bfloat16 or wider, within the bound.
A program may use at most 128 MiB of HBM per device.

v0:
```python
import jax
import jax.numpy as jnp
from jax import lax
from jax.sharding import PartitionSpec as P

HEAD_SIZE = 64
WINDOW_REACH = 128
NEG_LARGE = -1e30
NORM_EPS = 1e-05


def padded(block, sides, width):
    for axis, dim in sides:
        count = lax.axis_size(axis)
        forward = [(i, i + 1) for i in range(count - 1)]
        backward = [(target, source) for source, target in forward]
        low = lax.ppermute(
            lax.slice_in_dim(block, block.shape[dim] - width, None, axis=dim), axis, forward
        )
        high = lax.ppermute(lax.slice_in_dim(block, 0, width, axis=dim), axis, backward)
        block = jnp.concatenate([low, block, high], axis=dim)
    return block


def layer_norm(stream, gain_row):
    centre = jnp.mean(stream, axis=-1, keepdims=True)
    shifted = stream - centre
    spread = jnp.mean(shifted * shifted, axis=-1, keepdims=True)
    return shifted * lax.rsqrt(spread + NORM_EPS) * gain_row


def attend(queries, keyvals, head_sink_logit, doc_ids):
    tok_rows = queries.shape[0]
    kv_heads = keyvals.shape[1]
    heads_per_group = queries.shape[1] // (HEAD_SIZE * kv_heads)
    block_list = tok_rows // WINDOW_REACH
    score_scale = HEAD_SIZE ** (-0.5)
    doc_marks = doc_ids.astype(jnp.bfloat16)
    rim_keys, rim_docs = (
        padded(keyvals, (("sp", 0),), WINDOW_REACH),
        padded(doc_marks, (("sp", 0),), WINDOW_REACH),
    )
    padded_rows = rim_keys.reshape(block_list + 2, WINDOW_REACH, kv_heads, 2 * HEAD_SIZE)
    banded = jnp.concatenate([padded_rows[:-2], padded_rows[1:-1], padded_rows[2:]], axis=1)
    doc_ext = rim_docs.reshape(block_list + 2, WINDOW_REACH)
    doc_band = jnp.concatenate([doc_ext[:-2], doc_ext[1:-1], doc_ext[2:]], axis=1)
    offset = lax.axis_index("sp") * tok_rows
    total_rows = tok_rows * lax.axis_size("sp")
    query_pos = offset + jnp.arange(tok_rows, dtype=jnp.int32).reshape(block_list, WINDOW_REACH, 1)
    key_pos = (
        offset
        + (
            jnp.arange(block_list, dtype=jnp.int32)[:, None] * WINDOW_REACH
            + jnp.arange(3 * WINDOW_REACH, dtype=jnp.int32)[None, :]
            - WINDOW_REACH
        )[:, None, :]
    )
    allowed = (
        (jnp.abs(query_pos - key_pos) <= WINDOW_REACH)
        & (key_pos >= 0)
        & (key_pos < total_rows)
        & (doc_marks.reshape(block_list, WINDOW_REACH, 1) == doc_band[:, None, :])
    )
    query_block_list = queries.reshape(
        block_list, WINDOW_REACH, kv_heads, heads_per_group, HEAD_SIZE
    )
    scores = (
        jnp.einsum(
            "nqhgd,nkhd->nhgqk",
            query_block_list,
            banded[..., :HEAD_SIZE],
            preferred_element_type=jnp.float32,
        )
        * score_scale
    )
    scores = jnp.where(allowed[:, None, None], scores, NEG_LARGE)
    sink_col = head_sink_logit.reshape(kv_heads, heads_per_group)[None, :, :, None, None]
    highest = jnp.maximum(jnp.max(scores, axis=-1, keepdims=True), sink_col)
    powers = jnp.exp(scores - highest)
    denominator = jnp.sum(powers, axis=-1, keepdims=True) + jnp.exp(sink_col - highest)
    weights = (powers / denominator).astype(jnp.bfloat16)
    mixed_out = jnp.einsum(
        "nhgqk,nkhd->nqhgd", weights, banded[..., HEAD_SIZE:], preferred_element_type=jnp.float32
    )
    return mixed_out.astype(jnp.bfloat16).reshape(tok_rows, kv_heads * heads_per_group * HEAD_SIZE)


def per_device(
    queries,
    keyvals,
    head_sink_logit,
    doc_ids,
    stream_in,
    out_weight,
    first_gain,
    up_weight,
    down_weight,
    second_gain,
):
    up_whole = lax.all_gather(up_weight, "sp", axis=0, tiled=True)
    down_whole = lax.all_gather(down_weight, "sp", axis=1, tiled=True)
    attended = attend(queries, keyvals, head_sink_logit, doc_ids)
    tp_count = lax.axis_size("tp")
    own_rows = attended.shape[0] // tp_count
    by_peer = attended.reshape(tp_count, own_rows, attended.shape[1])
    projected = jnp.dot(
        lax.all_to_all(by_peer, "tp", split_axis=0, concat_axis=2, tiled=True)[0],
        out_weight,
        preferred_element_type=jnp.float32,
    )[None][0]
    first_stream = layer_norm(stream_in.astype(jnp.float32) + projected, first_gain).astype(
        jnp.bfloat16
    )
    hidden = jnp.dot(
        lax.all_gather(first_stream, "tp", axis=0, tiled=True),
        up_whole,
        preferred_element_type=jnp.float32,
    )
    active = jnp.square(jnp.maximum(hidden, 0.0)).astype(jnp.bfloat16)
    mixed_out = lax.psum_scatter(
        jnp.dot(active, down_whole, preferred_element_type=jnp.float32).astype(jnp.bfloat16),
        "tp",
        scatter_dimension=0,
        tiled=True,
    ).astype(jnp.float32)
    return layer_norm(first_stream.astype(jnp.float32) + mixed_out, second_gain).astype(
        jnp.bfloat16
    )


def solution(mesh):
    return jax.shard_map(
        per_device,
        mesh=mesh,
        in_specs=(
            P("sp", "tp"),
            P("sp", "tp", None),
            P("tp"),
            P("sp"),
            P(("sp", "tp"), None),
            P(),
            P(),
            P("sp", "tp"),
            P("tp", "sp"),
            P(),
        ),
        out_specs=P(("sp", "tp"), None),
        check_vma=False,
    )
```

profile of v0, /device:TPU:0, one launch (start us, length us, event | category | flops | bytes accessed | tf_op | source)
XLA Modules:
  0.0 477.8 jit_solution(12057201046544516895)
XLA Ops:
  6.5 0.0 all-gather.4.cloned.1.call-start
  6.5 0.8 convert_element_type.34
  7.3 2.4 collective-permute-start.2
  9.7 1.3 collective-permute-start.3
  11.0 1.4 copy.26
  12.4 5.8 %collective-permute-start = (bf16[128,4,128]{2,0,1:T(8,128)(2,1)S(1)}, bf16[128,4,128]{2,0,1:T(8,128)(2,1)}, u32[]{:S(2)}, u32[]{:S(2)}) collective-permute-start(bf16[128,4,128]{2,0,1:T(8,128)(2,1)S(1)} %get-tuple-element.7), channel_id=1, source_target_pairs={{0,2},{2,4},{4,6},{6,8},{8,10},{10,12},{12,14},{14,16},{16,18},{18... | collective-permute-start | bytes 393224 | tf_op jit(solution)/shard_map/ppermute | solution.py:17
  18.2 1.3 collective-permute-start.1
  19.5 0.7 convert_bitcast_fusion
  20.2 0.1 fusion.13
  20.3 0.1 add_add_fusion
  20.4 2.3 copy.32
  22.6 0.0 copy-done.7
  22.6 2.1 reshape.167
  24.7 0.0 copy-done.10
  24.7 0.1 max.24
  24.8 0.0 collective-permute-done.2
  24.8 0.0 collective-permute-done.3
  24.8 2.3 fusion.9
  27.1 0.0 collective-permute-done
  27.1 0.0 collective-permute-done.1
  27.1 1.3 pad_maximum_fusion.2
  28.4 0.7 copy.31
  29.1 0.7 copy.33
  29.7 0.0 copy-start.6
  29.7 1.8 pad_maximum_fusion
  31.6 0.1 copy-done.6
  31.6 2.5 fusion.1
  34.2 0.0 copy-done.4
  34.2 0.1 broadcast_maximum_fusion
  34.3 0.0 copy-start.5
  34.3 3.4 fusion
  37.7 0.1 exponential_add_fusion
  37.8 0.0 copy-done.5
  37.8 3.6 fusion.11
  41.4 0.7 copy.37
  42.1 0.4 reshape_reshape.3
  42.6 0.0 copy-start.3
  42.6 0.2 copy.38
  42.8 17.2 %all_to_all.15 = bf16[2,512,512]{1,2,0:T(8,128)(2,1)S(1)} all-to-all(bf16[2,512,512]{1,2,0:T(8,128)(2,1)S(1)} %copy.38), channel_id=1, replica_groups=mesh['sp'=16,'tp'=2] {'tp'}, dimensions={0} | all-to-all | bytes 2097152 | tf_op jit(solution)/shard_map/all_to_all | solution.py:107
  60.0 4.2 fusion.20
  64.2 0.0 copy-start.8
  64.2 0.6 multiply_reduce_fusion.1
  64.8 1.4 copy-done
  66.1 1.9 multiply_convert_fusion.2
  68.1 0.0 all-gather.4.cloned.1.call-update
  68.1 0.0 all-gather.6.cloned.1.call-start
  68.1 0.7 all-gather.6.cloned.1.call-update
  68.8 0.0 all-gather.8.cloned.1.call-start
  68.9 0.7 all-gather.8.cloned.1.call-update
  69.6 0.0 reduce-scatter.2.cloned.1.call-start
  69.6 56.9 %all-gather.4.cloned.1.call-done = bf16[1024,2048]{1,0:T(8,128)(2,1)} async-done(((bf16[512,2048]{1,0:T(8,128)(2,1)}), bf16[1024,2048]{1,0:T(8,128)(2,1)}) %all-gather.4.cloned.1.call-update) | async-done | bytes 4194320 | tf_op jit(solution)/shard_map/all_gather | solution.py:115
  126.5 128.6 %all-gather.6.cloned.1.call-done = bf16[2048,4096]{1,0:T(8,128)(2,1)} async-done(((bf16[128,4096]{1,0:T(8,128)(2,1)}), bf16[2048,4096]{1,0:T(8,128)(2,1)}) %all-gather.6.cloned.1.call-update) | async-done | bytes 16777232 | tf_op jit(solution)/shard_map/all_gather | solution.py:100
  255.1 22.9 %fusion.44 = bf16[1024,4096]{1,0:T(8,128)(2,1)} fusion(bf16[2048,4096]{1,0:T(8,128)(2,1)} %all-gather.6.cloned.1.call-done, bf16[1024,2048]{1,0:T(8,128)(2,1)} %all-gather.4.cloned.1.call-done), kind=kOutput, calls=%bitcast_fusion.1.clone.1 | convolution fusion | flops 17192452096 | bytes 29360128 | tf_op jit(solution)/shard_map/dot_general | solution.py:114
  278.0 107.4 %all-gather.8.cloned.1.call-done = bf16[4096,2048]{1,0:T(8,128)(2,1)} async-done(((bf16[4096,128]{1,0:T(8,128)(2,1)}), bf16[4096,2048]{1,0:T(8,128)(2,1)}) %all-gather.8.cloned.1.call-update) | async-done | bytes 16777232 | tf_op jit(solution)/shard_map/all_gather | solution.py:101
  385.4 23.7 %convolution_convert_fusion = bf16[1024,2048]{1,0:T(8,128)(2,1)} fusion(bf16[4096,2048]{1,0:T(8,128)(2,1)} %all-gather.8.cloned.1.call-done, bf16[1024,4096]{1,0:T(8,128)(2,1)} %fusion.44), kind=kOutput, calls=%fused_computation.15 | convolution fusion | flops 17181966336 | bytes 29360128 | tf_op jit(solution)/shard_map/dot_general | solution.py:121
  409.1 0.0 reduce-scatter.2.cloned.1.call-update
  409.1 52.7 %reduce-scatter.2.cloned.1.call-done = bf16[512,2048]{1,0:T(8,128)(2,1)} async-done(((bf16[1024,2048]{1,0:T(8,128)(2,1)}), bf16[512,2048]{1,0:T(8,128)(2,1)}) %reduce-scatter.2.cloned.1.call-update) | async-done | bytes 2097168 | tf_op jit(solution)/shard_map/reduce_scatter | solution.py:120
  461.8 3.9 fusion.4
  465.7 0.0 copy-start.9
  465.8 0.1 copy-done.1
  465.8 0.7 copy-done.2
  466.5 1.2 multiply_reduce_fusion
  467.8 0.0 copy-done.9
  467.8 3.5 multiply_convert_fusion.1
  (18 shorter events, 0.1 us)
Async XLA Ops:
  6.5 16.1 %copy-start.7 = (bf16[1024,512]{1,0:T(8,128)(2,1)S(1)}, bf16[1024,512]{1,0:T(8,128)(2,1)}, u32[]{:S(2)}) copy-start(bf16[1024,512]{1,0:T(8,128)(2,1)} %param.10) | copy-start | bytes 3145732
  6.5 18.2 %copy-start.10 = (f32[8]{0:T(128)S(1)}, f32[8]{0:T(128)}, u32[]{:S(2)}) copy-start(f32[8]{0:T(128)} %param.12) | copy-start | bytes 100
  6.5 119.9 %all-gather.4.cloned.1.call-start = ((), (), s32[]{:S(2)}) async-start(), calls=%async_computation.2 | async-start | bytes 6291456 | tf_op jit(solution)/shard_map/all_gather | solution.py:115
  7.3 17.5 %collective-permute-start.2 = (bf16[128]{0:T(256)(128)(2,1)S(1)}, bf16[128]{0:T(256)(128)(2,1)S(1)}, u32[]{:S(2)}, u32[]{:S(2)}) collective-permute-start(bf16[128]{0:T(256)(128)(2,1)S(1)} %get-tuple-element.11), channel_id=1, source_target_pairs={{0,2},{2,4},{4,6},{6,8},{8,10},{10,12},{12,14},{14,16},{16,18},{18... | collective-permute-start | bytes 776 | tf_op jit(solution)/shard_map/ppermute | solution.py:17
  9.7 15.1 %collective-permute-start.3 = (bf16[128]{0:T(256)(128)(2,1)S(1)}, bf16[128]{0:T(256)(128)(2,1)S(1)}, u32[]{:S(2)}, u32[]{:S(2)}) collective-permute-start(bf16[128]{0:T(256)(128)(2,1)S(1)} %get-tuple-element.12), channel_id=1, source_target_pairs={{2,0},{4,2},{6,4},{8,6},{10,8},{12,10},{14,12},{16,14},{18,16},{20... | collective-permute-start | bytes 776 | tf_op jit(solution)/shard_map/ppermute | solution.py:20
  12.4 14.7 %collective-permute-start = (bf16[128,4,128]{2,0,1:T(8,128)(2,1)S(1)}, bf16[128,4,128]{2,0,1:T(8,128)(2,1)}, u32[]{:S(2)}, u32[]{:S(2)}) collective-permute-start(bf16[128,4,128]{2,0,1:T(8,128)(2,1)S(1)} %get-tuple-element.7), channel_id=1, source_target_pairs={{0,2},{2,4},{4,6},{6,8},{8,10},{10,12},{12,14},{14,16},{16,18},{18... | collective-permute-start | bytes 393224 | tf_op jit(solution)/shard_map/ppermute | solution.py:17
  18.2 8.9 %collective-permute-start.1 = (bf16[128,4,128]{2,0,1:T(8,128)(2,1)S(1)}, bf16[128,4,128]{2,0,1:T(8,128)(2,1)}, u32[]{:S(2)}, u32[]{:S(2)}) collective-permute-start(bf16[128,4,128]{2,0,1:T(8,128)(2,1)S(1)} %get-tuple-element.8), channel_id=1, source_target_pairs={{2,0},{4,2},{6,4},{8,6},{10,8},{12,10},{14,12},{16,14},{18,16},{20... | collective-permute-start | bytes 393224 | tf_op jit(solution)/shard_map/ppermute | solution.py:20
  29.7 1.9 copy-start.6
  31.6 2.5 copy-start.4
  34.3 3.6 copy-start.5
  42.6 17.4 %copy-start.3 = (bf16[1024,2048]{1,0:T(8,128)(2,1)S(1)}, bf16[1024,2048]{1,0:T(8,128)(2,1)}, u32[]{:S(2)}) copy-start(bf16[1024,2048]{1,0:T(8,128)(2,1)} %param.15) | copy-start | bytes 12582916
  64.2 1.9 copy-start
  64.2 1.9 copy-start.8
  68.1 187.0 %all-gather.6.cloned.1.call-start = ((), (), s32[]{:S(2)}) async-start(), calls=%async_computation.3 | async-start | bytes 17825792 | tf_op jit(solution)/shard_map/all_gather | solution.py:100
  68.8 316.5 %all-gather.8.cloned.1.call-start = ((), (), s32[]{:S(2)}) async-start(), calls=%async_computation.4 | async-start | bytes 17825792 | tf_op jit(solution)/shard_map/all_gather | solution.py:101
  69.6 392.2 %reduce-scatter.2.cloned.1.call-start = ((), (), s32[]{:S(2)}) async-start(), calls=%async_computation.5 | async-start | bytes 6291456 | tf_op jit(solution)/shard_map/reduce_scatter | solution.py:120
  461.8 4.0 copy-start.1
  461.8 4.7 copy-start.2
  465.7 2.0 copy-start.9
Sparse Core Ops, SparseCore 0:
  68.2 58.2 all-gather.3
  128.6 126.4 all-gather.5
  257.3 128.0 all-gather.7
  409.2 52.5 reduce-scatter.1
where the time goes:
time: 478 us
  waiting for transfers between devices  347 us (73%)
  matrix products  56.9 us (12%)
  other arithmetic  21.8 us (5%)
  blocking collectives  17.2 us (4%)
  between operations  13.4 us (3%)
  starting transfers between devices  10.9 us (2%)
  local copies, waits for them, and re-layouts  10.6 us (2%)
    all_gather x1, waiting for transfers between devices, per_device(): up_whole = lax.all_gather(up_weight, 'sp', axis=0, tiled=True)  129 us
    all_gather x1, waiting for transfers between devices, per_device(): down_whole = lax.all_gather(down_weight, 'sp', axis=1, tiled=True)  107 us
    all_gather x1, waiting for transfers between devices, per_device(): lax.all_gather(first_stream, 'tp', axis=0, tiled=True)  56.9 us
    reduce_scatter x1, waiting for transfers between devices, per_device(): lax.psum_scatter(jnp.dot(active, down_whole, preferred_element_type=jnp.f...  52.7 us
    dot_general x1, matrix products, per_device(): jnp.dot(active, down_whole, preferred_element_type=jnp.float32)  23.7 us
    dot_general x1, matrix products, per_device(): jnp.dot(lax.all_gather(first_stream, 'tp', axis=0, tiled=True), up_whole,...  22.9 us
    all_to_all x1, blocking collectives, per_device(): lax.all_to_all(by_peer, 'tp', split_axis=0, concat_axis=2, tiled=True)[0]  17.2 us
  transfers between devices with their start and end apart: 8, of which 4 were waited for; matrix products, arithmetic and copies ran while one was open for 7% of the time, Pallas kernels for 0%

commit v1 on v0

--- a/solution.py
+++ b/solution.py
@@ -98,7 +98,12 @@
     second_gain,
 ):
     up_whole = lax.all_gather(up_weight, "sp", axis=0, tiled=True)
-    down_whole = lax.all_gather(down_weight, "sp", axis=1, tiled=True)
+    ring = [down_weight]
+    for hop in range(15):
+        ring.append(lax.ppermute(ring[-1], "sp", [(dev, (dev + 1) % 16) for dev in range(16)]))
+    down_whole = jnp.roll(
+        jnp.concatenate(ring[::-1], axis=1), (lax.axis_index("sp") + 1) * ring[0].shape[1], axis=1
+    )
     attended = attend(queries, keyvals, head_sink_logit, doc_ids)
     tp_count = lax.axis_size("tp")
     own_rows = attended.shape[0] // tp_count

time: 478 us -> 575 us (1.20)
  local copies, waits for them, and re-layouts: 10.6 us -> 72.1 us
  waiting for transfers between devices: 347 us -> 380 us
    ppermute x0 -> x15, waiting for transfers between devices: none -> 328 us  [per_device(): lax.ppermute(ring[-1], 'sp', [(dev, (dev + 1) % 16) for dev in range(16)])]
    all_gather x1, waiting for transfers between devices: 129 us -> 0.01 us  [per_device(): up_whole = lax.all_gather(up_weight, 'sp', axis=0, tiled=True)]
    all_gather x1 -> x0, waiting for transfers between devices: 107 us -> none  [per_device(): down_whole = lax.all_gather(down_weight, 'sp', axis=1, tiled=True)]
    all_gather x1, waiting for transfers between devices: 56.9 us -> 0.01 us  [per_device(): lax.all_gather(first_stream, 'tp', axis=0, tiled=True)]
    unnamed x23 -> x92, local copies, waits for them, and re-layouts: 3.57 us -> 60 us
  transfers between devices with their start and end apart: 8 -> 22, of which waited for: 4 -> 16; matrix products, arithmetic and copies ran while one was open for 7% -> 10% of each run, Pallas kernels for 0% -> 0%
where the time goes in v1:
time: 575 us
  waiting for transfers between devices  380 us (66%)
  local copies, waits for them, and re-layouts  72.1 us (13%)
  matrix products  57.2 us (10%)
  other arithmetic  24.6 us (4%)
  blocking collectives  16.3 us (3%)
  between operations  13.4 us (2%)
  starting transfers between devices  11.4 us (2%)
    ppermute x15, waiting for transfers between devices, per_device(): lax.ppermute(ring[-1], 'sp', [(dev, (dev + 1) % 16) for dev in range(16)])  328 us
    unnamed x92, local copies, waits for them, and re-layouts  60 us
    reduce_scatter x1, waiting for transfers between devices, per_device(): lax.psum_scatter(jnp.dot(active, down_whole, preferred_element_type=jnp.f...  51.1 us
    dot_general x1, matrix products, per_device(): jnp.dot(lax.all_gather(first_stream, 'tp', axis=0, tiled=True), up_whole,...  21.5 us
    dot_general x1, matrix products, per_device(): jnp.dot(active, down_whole, preferred_element_type=jnp.float32)  21.3 us
    all_to_all x1, blocking collectives, per_device(): lax.all_to_all(by_peer, 'tp', split_axis=0, concat_axis=2, tiled=True)[0]  16.3 us
  transfers between devices with their start and end apart: 22, of which 16 were waited for; matrix products, arithmetic and copies ran while one was open for 10% of the time, Pallas kernels for 0%

profile of v1, /device:TPU:0, one launch (start us, length us, event | category | flops | bytes accessed | tf_op | source)
XLA Modules:
  0.0 574.6 jit_solution(10261648843819467497)
XLA Ops:
  7.2 2.4 collective-permute-start.2
  9.6 1.3 collective-permute-start.3
  10.9 1.4 copy.26
  12.3 5.2 collective-permute-start
  17.5 1.3 collective-permute-start.1
  19.7 2.3 copy.32
  21.9 5.3 reshape.167
  28.0 2.3 fusion.14
  31.0 1.2 pad_maximum_fusion.2
  33.6 1.7 pad_maximum_fusion
  35.3 1.6 copy-done.26
  37.0 4.0 fusion.3
  41.0 3.6 fusion.2
  44.7 4.9 fusion.16
  50.9 16.3 %all_to_all.15 = bf16[2,512,512]{1,2,0:T(8,128)(2,1)S(1)} all-to-all(bf16[2,512,512]{1,2,0:T(8,128)(2,1)S(1)} %copy.38), channel_id=1, replica_groups=mesh['sp'=16,'tp'=2] {'tp'}, dimensions={0} | all-to-all | bytes 2097152 | tf_op jit(solution)/shard_map/all_to_all | solution.py:112
  67.2 5.6 fusion.26
  73.3 1.5 copy-done
  74.8 1.9 multiply_convert_fusion.2
  77.6 1.2 collective-permute-start.4
  78.8 16.1 %collective-permute-done.4 = bf16[4096,128]{1,0:T(8,128)(2,1)S(1)} collective-permute-done((bf16[4096,128]{1,0:T(8,128)(2,1)S(1)}, bf16[4096,128]{1,0:T(8,128)(2,1)S(1)}, u32[]{:S(2)}, u32[]{:S(2)}) %collective-permute-start.4) | collective-permute-done | bytes 1048608 | tf_op jit(solution)/shard_map/ppermute | solution.py:103
  94.8 16.9 %collective-permute-done.5 = bf16[4096,128]{1,0:T(8,128)(2,1)S(1)} collective-permute-done((bf16[4096,128]{1,0:T(8,128)(2,1)S(1)}, bf16[4096,128]{1,0:T(8,128)(2,1)S(1)}, u32[]{:S(2)}, u32[]{:S(2)}) %collective-permute-start.5) | collective-permute-done | bytes 1048608 | tf_op jit(solution)/shard_map/ppermute | solution.py:103
  111.8 16.9 %collective-permute-done.6 = bf16[4096,128]{1,0:T(8,128)(2,1)S(1)} collective-permute-done((bf16[4096,128]{1,0:T(8,128)(2,1)S(1)}, bf16[4096,128]{1,0:T(8,128)(2,1)S(1)}, u32[]{:S(2)}, u32[]{:S(2)}) %collective-permute-start.6) | collective-permute-done | bytes 1048608 | tf_op jit(solution)/shard_map/ppermute | solution.py:103
  129.7 16.9 %collective-permute-done.7 = bf16[4096,128]{1,0:T(8,128)(2,1)S(1)} collective-permute-done((bf16[4096,128]{1,0:T(8,128)(2,1)S(1)}, bf16[4096,128]{1,0:T(8,128)(2,1)S(1)}, u32[]{:S(2)}, u32[]{:S(2)}) %collective-permute-start.7) | collective-permute-done | bytes 1048608 | tf_op jit(solution)/shard_map/ppermute | solution.py:103
  147.5 39.3 %collective-permute-done.8 = bf16[4096,128]{1,0:T(8,128)(2,1)S(1)} collective-permute-done((bf16[4096,128]{1,0:T(8,128)(2,1)S(1)}, bf16[4096,128]{1,0:T(8,128)(2,1)S(1)}, u32[]{:S(2)}, u32[]{:S(2)}) %collective-permute-start.8) | collective-permute-done | bytes 1048608 | tf_op jit(solution)/shard_map/ppermute | solution.py:103
  187.8 23.6 %collective-permute-done.9 = bf16[4096,128]{1,0:T(8,128)(2,1)S(1)} collective-permute-done((bf16[4096,128]{1,0:T(8,128)(2,1)S(1)}, bf16[4096,128]{1,0:T(8,128)(2,1)S(1)}, u32[]{:S(2)}, u32[]{:S(2)}) %collective-permute-start.9) | collective-permute-done | bytes 1048608 | tf_op jit(solution)/shard_map/ppermute | solution.py:103
  212.4 39.5 %collective-permute-done.10 = bf16[4096,128]{1,0:T(8,128)(2,1)S(1)} collective-permute-done((bf16[4096,128]{1,0:T(8,128)(2,1)S(1)}, bf16[4096,128]{1,0:T(8,128)(2,1)S(1)}, u32[]{:S(2)}, u32[]{:S(2)}) %collective-permute-start.10) | collective-permute-done | bytes 1048608 | tf_op jit(solution)/shard_map/ppermute | solution.py:103
  252.9 38.5 %collective-permute-done.11 = bf16[4096,128]{1,0:T(8,128)(2,1)S(1)} collective-permute-done((bf16[4096,128]{1,0:T(8,128)(2,1)S(1)}, bf16[4096,128]{1,0:T(8,128)(2,1)S(1)}, u32[]{:S(2)}, u32[]{:S(2)}) %collective-permute-start.11) | collective-permute-done | bytes 1048608 | tf_op jit(solution)/shard_map/ppermute | solution.py:103
  292.3 18.2 %collective-permute-done.12 = bf16[4096,128]{1,0:T(8,128)(2,1)S(1)} collective-permute-done((bf16[4096,128]{1,0:T(8,128)(2,1)S(1)}, bf16[4096,128]{1,0:T(8,128)(2,1)S(1)}, u32[]{:S(2)}, u32[]{:S(2)}) %collective-permute-start.12) | collective-permute-done | bytes 1048608 | tf_op jit(solution)/shard_map/ppermute | solution.py:103
  311.5 16.9 %collective-permute-done.13 = bf16[4096,128]{1,0:T(8,128)(2,1)S(1)} collective-permute-done((bf16[4096,128]{1,0:T(8,128)(2,1)S(1)}, bf16[4096,128]{1,0:T(8,128)(2,1)S(1)}, u32[]{:S(2)}, u32[]{:S(2)}) %collective-permute-start.13) | collective-permute-done | bytes 1048608 | tf_op jit(solution)/shard_map/ppermute | solution.py:103
  329.5 16.9 %collective-permute-done.14 = bf16[4096,128]{1,0:T(8,128)(2,1)S(1)} collective-permute-done((bf16[4096,128]{1,0:T(8,128)(2,1)S(1)}, bf16[4096,128]{1,0:T(8,128)(2,1)S(1)}, u32[]{:S(2)}, u32[]{:S(2)}) %collective-permute-start.14) | collective-permute-done | bytes 1048608 | tf_op jit(solution)/shard_map/ppermute | solution.py:103
  347.4 16.9 %collective-permute-done.15 = bf16[4096,128]{1,0:T(8,128)(2,1)S(1)} collective-permute-done((bf16[4096,128]{1,0:T(8,128)(2,1)S(1)}, bf16[4096,128]{1,0:T(8,128)(2,1)S(1)}, u32[]{:S(2)}, u32[]{:S(2)}) %collective-permute-start.15) | collective-permute-done | bytes 1048608 | tf_op jit(solution)/shard_map/ppermute | solution.py:103
  365.2 16.9 %collective-permute-done.16 = bf16[4096,128]{1,0:T(8,128)(2,1)S(1)} collective-permute-done((bf16[4096,128]{1,0:T(8,128)(2,1)S(1)}, bf16[4096,128]{1,0:T(8,128)(2,1)S(1)}, u32[]{:S(2)}, u32[]{:S(2)}) %collective-permute-start.16) | collective-permute-done | bytes 1048608 | tf_op jit(solution)/shard_map/ppermute | solution.py:103
  383.2 17.0 %collective-permute-done.17 = bf16[4096,128]{1,0:T(8,128)(2,1)} collective-permute-done((bf16[4096,128]{1,0:T(8,128)(2,1)S(1)}, bf16[4096,128]{1,0:T(8,128)(2,1)}, u32[]{:S(2)}, u32[]{:S(2)}) %collective-permute-start.17) | collective-permute-done | bytes 1048608 | tf_op jit(solution)/shard_map/ppermute | solution.py:103
  400.2 17.2 %collective-permute-done.18 = bf16[4096,128]{1,0:T(8,128)(2,1)} collective-permute-done((bf16[4096,128]{1,0:T(8,128)(2,1)}, bf16[4096,128]{1,0:T(8,128)(2,1)}, u32[]{:S(2)}, u32[]{:S(2)}) %collective-permute-start.18) | collective-permute-done | bytes 1048608 | tf_op jit(solution)/shard_map/ppermute | solution.py:103
  417.4 2.3 constant_dynamic-update-slice_fusion.31
  419.7 2.3 constant_dynamic-update-slice_fusion.30
  422.1 2.3 constant_dynamic-update-slice_fusion.29
  424.4 2.3 constant_dynamic-update-slice_fusion.28
  426.7 2.3 constant_dynamic-update-slice_fusion.27
  429.0 2.3 constant_dynamic-update-slice_fusion.26
  432.4 1.1 constant_dynamic-update-slice_fusion.24
  433.5 1.1 constant_dynamic-update-slice_fusion.23
  434.6 1.1 constant_dynamic-update-slice_fusion.22
  435.7 1.1 constant_dynamic-update-slice_fusion.21
  436.8 1.1 constant_dynamic-update-slice_fusion.20
  438.0 1.1 constant_dynamic-update-slice_fusion.19
  439.1 1.1 constant_dynamic-update-slice_fusion.18
  440.2 1.1 constant_dynamic-update-slice_fusion.17
  442.4 2.3 constant_dynamic-update-slice_fusion.15
  444.7 2.3 constant_dynamic-update-slice_fusion.14
  447.1 1.1 constant_dynamic-update-slice_fusion.13
  448.2 1.1 constant_dynamic-update-slice_fusion.12
  449.3 1.1 constant_dynamic-update-slice_fusion.11
  450.4 1.1 constant_dynamic-update-slice_fusion.10
  451.5 1.2 constant_dynamic-update-slice_fusion.9
  452.7 1.1 constant_dynamic-update-slice_fusion.8
  457.1 1.1 constant_dynamic-update-slice_fusion.4
  460.4 1.1 constant_dynamic-update-slice_fusion.1
  462.5 21.5 %fusion.54 = bf16[1024,4096]{1,0:T(8,128)(2,1)S(1)} fusion(bf16[2048,4096]{1,0:T(8,128)(2,1)} %all-gather.5.cloned.1.call-done, bf16[1024,2048]{1,0:T(8,128)(2,1)} %all-gather.3.cloned.1.call-done), kind=kOutput, calls=%bitcast_fusion.1.clone.2 | convolution fusion | flops 17192452096 | bytes 29360128 | tf_op jit(solution)/shard_map/dot_general | solution.py:119
  484.1 21.3 %fusion.7 = bf16[1024,2048]{1,0:T(8,128)(2,1)} fusion(bf16[4096,4096]{1,0:T(8,128)(2,1)} %constant_dynamic-update-slice_fusion, s32[]{:T(128)S(6)} %select_n.19, bf16[1024,4096]{1,0:T(8,128)(2,1)S(1)} %fusion.54), kind=kOutput, calls=%fused_computation.17 | convolution fusion | flops 17181966336 | bytes 29360132 | tf_op jit(solution)/shard_map/dot_general | solution.py:126
  505.3 51.1 %reduce-scatter.2.cloned.1.call-done = bf16[512,2048]{1,0:T(8,128)(2,1)} async-done(((bf16[1024,2048]{1,0:T(8,128)(2,1)}), bf16[512,2048]{1,0:T(8,128)(2,1)}) %reduce-scatter.2.cloned.1.call-update) | async-done | bytes 2097168 | tf_op jit(solution)/shard_map/reduce_scatter | solution.py:125
  556.5 3.9 fusion.6
  560.4 4.1 multiply_reduce_fusion
  564.5 3.5 multiply_convert_fusion.1
  (115 shorter events, 26.7 us)
Async XLA Ops:
  6.5 456.0 %all-gather.3.cloned.1.call-start = ((), (), s32[]{:S(2)}) async-start(), calls=%async_computation.2 | async-start | bytes 6291456 | tf_op jit(solution)/shard_map/all_gather | solution.py:120
  7.2 20.8 %collective-permute-start.2 = (bf16[128]{0:T(256)(128)(2,1)S(1)}, bf16[128]{0:T(256)(128)(2,1)S(1)}, u32[]{:S(2)}, u32[]{:S(2)}) collective-permute-start(bf16[128]{0:T(256)(128)(2,1)S(1)} %get-tuple-element.11), channel_id=1, source_target_pairs={{0,2},{2,4},{4,6},{6,8},{8,10},{10,12},{12,14},{14,16},{16,18},{18... | collective-permute-start | bytes 776 | tf_op jit(solution)/shard_map/ppermute | solution.py:17
  9.6 18.4 %collective-permute-start.3 = (bf16[128]{0:T(256)(128)(2,1)S(1)}, bf16[128]{0:T(256)(128)(2,1)S(1)}, u32[]{:S(2)}, u32[]{:S(2)}) collective-permute-start(bf16[128]{0:T(256)(128)(2,1)S(1)} %get-tuple-element.12), channel_id=1, source_target_pairs={{2,0},{4,2},{6,4},{8,6},{10,8},{12,10},{14,12},{16,14},{18,16},{20... | collective-permute-start | bytes 776 | tf_op jit(solution)/shard_map/ppermute | solution.py:20
  12.3 18.0 %collective-permute-start = (bf16[128,4,128]{2,0,1:T(8,128)(2,1)S(1)}, bf16[128,4,128]{2,0,1:T(8,128)(2,1)S(1)}, u32[]{:S(2)}, u32[]{:S(2)}) collective-permute-start(bf16[128,4,128]{2,0,1:T(8,128)(2,1)S(1)} %get-tuple-element.7), channel_id=1, source_target_pairs={{0,2},{2,4},{4,6},{6,8},{8,10},{10,12},{12,14},{14,16},{16,18},{18... | collective-permute-start | bytes 393224 | tf_op jit(solution)/shard_map/ppermute | solution.py:17
  17.5 13.5 %collective-permute-start.1 = (bf16[128,4,128]{2,0,1:T(8,128)(2,1)S(1)}, bf16[128,4,128]{2,0,1:T(8,128)(2,1)}, u32[]{:S(2)}, u32[]{:S(2)}) collective-permute-start(bf16[128,4,128]{2,0,1:T(8,128)(2,1)S(1)} %get-tuple-element.8), channel_id=1, source_target_pairs={{2,0},{4,2},{6,4},{8,6},{10,8},{12,10},{14,12},{16,14},{18,16},{20... | collective-permute-start | bytes 393224 | tf_op jit(solution)/shard_map/ppermute | solution.py:20
  30.4 0.7 copy-start.28
  35.3 1.6 copy-start.26
  49.6 25.2 %copy-start.27 = (f32[2048]{0:T(1024)S(1)}, f32[2048]{0:T(1024)}, u32[]{:S(2)}) copy-start(f32[2048]{0:T(1024)} %param.16) | copy-start | bytes 24580
  67.2 10.4 %copy-start.3 = (bf16[4096,128]{1,0:T(8,128)(2,1)S(1)}, bf16[4096,128]{1,0:T(8,128)(2,1)}, u32[]{:S(2)}) copy-start(bf16[4096,128]{1,0:T(8,128)(2,1)} %param.18) | copy-start | bytes 3145732
  72.8 2.1 copy-start
  76.8 385.8 %all-gather.5.cloned.1.call-start = ((), (), s32[]{:S(2)}) async-start(), calls=%async_computation.3 | async-start | bytes 17825792 | tf_op jit(solution)/shard_map/all_gather | solution.py:100
  77.5 478.9 %reduce-scatter.2.cloned.1.call-start = ((), (), s32[]{:S(2)}) async-start(), calls=%async_computation.4 | async-start | bytes 6291456 | tf_op jit(solution)/shard_map/reduce_scatter | solution.py:125
  77.6 17.3 %collective-permute-start.4 = (bf16[4096,128]{1,0:T(8,128)(2,1)S(1)}, bf16[4096,128]{1,0:T(8,128)(2,1)S(1)}, u32[]{:S(2)}, u32[]{:S(2)}) collective-permute-start(bf16[4096,128]{1,0:T(8,128)(2,1)S(1)} %copy-done.3), channel_id=1, source_target_pairs={{0,2},{2,4},{4,6},{6,8},{8,10},{10,12},{12,14},{14,16},{16,18},{18... | collective-permute-start | bytes 3145736 | tf_op jit(solution)/shard_map/ppermute | solution.py:103
  94.8 16.9 %collective-permute-start.5 = (bf16[4096,128]{1,0:T(8,128)(2,1)S(1)}, bf16[4096,128]{1,0:T(8,128)(2,1)S(1)}, u32[]{:S(2)}, u32[]{:S(2)}) collective-permute-start(bf16[4096,128]{1,0:T(8,128)(2,1)S(1)} %collective-permute-done.4), channel_id=1, source_target_pairs={{0,2},{2,4},{4,6},{6,8},{8,10},{10,12},{12,14},{14,16},{16,18},{18... | collective-permute-start | bytes 3145736 | tf_op jit(solution)/shard_map/ppermute | solution.py:103
  111.8 16.9 %collective-permute-start.6 = (bf16[4096,128]{1,0:T(8,128)(2,1)S(1)}, bf16[4096,128]{1,0:T(8,128)(2,1)S(1)}, u32[]{:S(2)}, u32[]{:S(2)}) collective-permute-start(bf16[4096,128]{1,0:T(8,128)(2,1)S(1)} %collective-permute-done.5), channel_id=1, source_target_pairs={{0,2},{2,4},{4,6},{6,8},{8,10},{10,12},{12,14},{14,16},{16,18},{18... | collective-permute-start | bytes 3145736 | tf_op jit(solution)/shard_map/ppermute | solution.py:103
  128.7 1.0 copy-start.4
  129.7 16.9 %collective-permute-start.7 = (bf16[4096,128]{1,0:T(8,128)(2,1)S(1)}, bf16[4096,128]{1,0:T(8,128)(2,1)S(1)}, u32[]{:S(2)}, u32[]{:S(2)}) collective-permute-start(bf16[4096,128]{1,0:T(8,128)(2,1)S(1)} %collective-permute-done.6), channel_id=1, source_target_pairs={{0,2},{2,4},{4,6},{6,8},{8,10},{10,12},{12,14},{14,16},{16,18},{18... | collective-permute-start | bytes 3145736 | tf_op jit(solution)/shard_map/ppermute | solution.py:103
  146.6 1.0 copy-start.6
  147.5 39.3 %collective-permute-start.8 = (bf16[4096,128]{1,0:T(8,128)(2,1)S(1)}, bf16[4096,128]{1,0:T(8,128)(2,1)S(1)}, u32[]{:S(2)}, u32[]{:S(2)}) collective-permute-start(bf16[4096,128]{1,0:T(8,128)(2,1)S(1)} %collective-permute-done.7), channel_id=1, source_target_pairs={{0,2},{2,4},{4,6},{6,8},{8,10},{10,12},{12,14},{14,16},{16,18},{18... | collective-permute-start | bytes 3145736 | tf_op jit(solution)/shard_map/ppermute | solution.py:103
  186.8 1.0 copy-start.8
  187.8 23.6 %collective-permute-start.9 = (bf16[4096,128]{1,0:T(8,128)(2,1)S(1)}, bf16[4096,128]{1,0:T(8,128)(2,1)S(1)}, u32[]{:S(2)}, u32[]{:S(2)}) collective-permute-start(bf16[4096,128]{1,0:T(8,128)(2,1)S(1)} %collective-permute-done.8), channel_id=1, source_target_pairs={{0,2},{2,4},{4,6},{6,8},{8,10},{10,12},{12,14},{14,16},{16,18},{18... | collective-permute-start | bytes 3145736 | tf_op jit(solution)/shard_map/ppermute | solution.py:103
  211.4 1.0 copy-start.10
  212.4 39.5 %collective-permute-start.10 = (bf16[4096,128]{1,0:T(8,128)(2,1)S(1)}, bf16[4096,128]{1,0:T(8,128)(2,1)S(1)}, u32[]{:S(2)}, u32[]{:S(2)}) collective-permute-start(bf16[4096,128]{1,0:T(8,128)(2,1)S(1)} %collective-permute-done.9), channel_id=1, source_target_pairs={{0,2},{2,4},{4,6},{6,8},{8,10},{10,12},{12,14},{14,16},{16,18},{18... | collective-permute-start | bytes 3145736 | tf_op jit(solution)/shard_map/ppermute | solution.py:103
  251.9 1.0 copy-start.12
  252.9 38.5 %collective-permute-start.11 = (bf16[4096,128]{1,0:T(8,128)(2,1)S(1)}, bf16[4096,128]{1,0:T(8,128)(2,1)S(1)}, u32[]{:S(2)}, u32[]{:S(2)}) collective-permute-start(bf16[4096,128]{1,0:T(8,128)(2,1)S(1)} %collective-permute-done.10), channel_id=1, source_target_pairs={{0,2},{2,4},{4,6},{6,8},{8,10},{10,12},{12,14},{14,16},{16,18},{18... | collective-permute-start | bytes 3145736 | tf_op jit(solution)/shard_map/ppermute | solution.py:103
  291.3 1.0 copy-start.14
  292.3 18.2 %collective-permute-start.12 = (bf16[4096,128]{1,0:T(8,128)(2,1)S(1)}, bf16[4096,128]{1,0:T(8,128)(2,1)S(1)}, u32[]{:S(2)}, u32[]{:S(2)}) collective-permute-start(bf16[4096,128]{1,0:T(8,128)(2,1)S(1)} %collective-permute-done.11), channel_id=1, source_target_pairs={{0,2},{2,4},{4,6},{6,8},{8,10},{10,12},{12,14},{14,16},{16,18},{18... | collective-permute-start | bytes 3145736 | tf_op jit(solution)/shard_map/ppermute | solution.py:103
  310.5 1.0 copy-start.16
  311.5 16.9 %collective-permute-start.13 = (bf16[4096,128]{1,0:T(8,128)(2,1)S(1)}, bf16[4096,128]{1,0:T(8,128)(2,1)S(1)}, u32[]{:S(2)}, u32[]{:S(2)}) collective-permute-start(bf16[4096,128]{1,0:T(8,128)(2,1)S(1)} %collective-permute-done.12), channel_id=1, source_target_pairs={{0,2},{2,4},{4,6},{6,8},{8,10},{10,12},{12,14},{14,16},{16,18},{18... | collective-permute-start | bytes 3145736 | tf_op jit(solution)/shard_map/ppermute | solution.py:103
  328.5 1.0 copy-start.18
  329.5 16.9 %collective-permute-start.14 = (bf16[4096,128]{1,0:T(8,128)(2,1)S(1)}, bf16[4096,128]{1,0:T(8,128)(2,1)S(1)}, u32[]{:S(2)}, u32[]{:S(2)}) collective-permute-start(bf16[4096,128]{1,0:T(8,128)(2,1)S(1)} %collective-permute-done.13), channel_id=1, source_target_pairs={{0,2},{2,4},{4,6},{6,8},{8,10},{10,12},{12,14},{14,16},{16,18},{18... | collective-permute-start | bytes 3145736 | tf_op jit(solution)/shard_map/ppermute | solution.py:103
  346.4 1.0 copy-start.20
  347.4 16.9 %collective-permute-start.15 = (bf16[4096,128]{1,0:T(8,128)(2,1)S(1)}, bf16[4096,128]{1,0:T(8,128)(2,1)S(1)}, u32[]{:S(2)}, u32[]{:S(2)}) collective-permute-start(bf16[4096,128]{1,0:T(8,128)(2,1)S(1)} %collective-permute-done.14), channel_id=1, source_target_pairs={{0,2},{2,4},{4,6},{6,8},{8,10},{10,12},{12,14},{14,16},{16,18},{18... | collective-permute-start | bytes 3145736 | tf_op jit(solution)/shard_map/ppermute | solution.py:103
  364.3 1.0 copy-start.22
  365.2 16.9 %collective-permute-start.16 = (bf16[4096,128]{1,0:T(8,128)(2,1)S(1)}, bf16[4096,128]{1,0:T(8,128)(2,1)S(1)}, u32[]{:S(2)}, u32[]{:S(2)}) collective-permute-start(bf16[4096,128]{1,0:T(8,128)(2,1)S(1)} %collective-permute-done.15), channel_id=1, source_target_pairs={{0,2},{2,4},{4,6},{6,8},{8,10},{10,12},{12,14},{14,16},{16,18},{18... | collective-permute-start | bytes 3145736 | tf_op jit(solution)/shard_map/ppermute | solution.py:103
  382.2 1.0 copy-start.24
  383.2 17.0 %collective-permute-start.17 = (bf16[4096,128]{1,0:T(8,128)(2,1)S(1)}, bf16[4096,128]{1,0:T(8,128)(2,1)}, u32[]{:S(2)}, u32[]{:S(2)}) collective-permute-start(bf16[4096,128]{1,0:T(8,128)(2,1)S(1)} %collective-permute-done.16), channel_id=1, source_target_pairs={{0,2},{2,4},{4,6},{6,8},{8,10},{10,12},{12,14},{14,16},{16,18},{18... | collective-permute-start | bytes 3145736 | tf_op jit(solution)/shard_map/ppermute | solution.py:103
  400.2 17.2 %collective-permute-start.18 = (bf16[4096,128]{1,0:T(8,128)(2,1)}, bf16[4096,128]{1,0:T(8,128)(2,1)}, u32[]{:S(2)}, u32[]{:S(2)}) collective-permute-start(bf16[4096,128]{1,0:T(8,128)(2,1)} %collective-permute-done.17), channel_id=1, source_target_pairs={{0,2},{2,4},{4,6},{6,8},{8,10},{10,12},{12,14},{14,16},{16,18},{18... | collective-permute-start | bytes 3145736 | tf_op jit(solution)/shard_map/ppermute | solution.py:103
  400.2 31.1 %copy-start.17 = (bf16[4096,128]{1,0:T(8,128)(2,1)S(1)}, bf16[4096,128]{1,0:T(8,128)(2,1)}, u32[]{:S(2)}) copy-start(bf16[4096,128]{1,0:T(8,128)(2,1)} %copy-done.16) | copy-start | bytes 3145732
  400.2 32.2 %copy-start.15 = (bf16[4096,128]{1,0:T(8,128)(2,1)S(1)}, bf16[4096,128]{1,0:T(8,128)(2,1)}, u32[]{:S(2)}) copy-start(bf16[4096,128]{1,0:T(8,128)(2,1)} %copy-done.14) | copy-start | bytes 3145732
  400.2 33.3 %copy-start.13 = (bf16[4096,128]{1,0:T(8,128)(2,1)S(1)}, bf16[4096,128]{1,0:T(8,128)(2,1)}, u32[]{:S(2)}) copy-start(bf16[4096,128]{1,0:T(8,128)(2,1)} %copy-done.12) | copy-start | bytes 3145732
  400.2 34.4 %copy-start.11 = (bf16[4096,128]{1,0:T(8,128)(2,1)S(1)}, bf16[4096,128]{1,0:T(8,128)(2,1)}, u32[]{:S(2)}) copy-start(bf16[4096,128]{1,0:T(8,128)(2,1)} %copy-done.10) | copy-start | bytes 3145732
  400.2 35.5 %copy-start.9 = (bf16[4096,128]{1,0:T(8,128)(2,1)S(1)}, bf16[4096,128]{1,0:T(8,128)(2,1)}, u32[]{:S(2)}) copy-start(bf16[4096,128]{1,0:T(8,128)(2,1)} %copy-done.8) | copy-start | bytes 3145732
  400.2 36.6 %copy-start.7 = (bf16[4096,128]{1,0:T(8,128)(2,1)S(1)}, bf16[4096,128]{1,0:T(8,128)(2,1)}, u32[]{:S(2)}) copy-start(bf16[4096,128]{1,0:T(8,128)(2,1)} %copy-done.6) | copy-start | bytes 3145732
  400.2 37.7 %copy-start.5 = (bf16[4096,128]{1,0:T(8,128)(2,1)S(1)}, bf16[4096,128]{1,0:T(8,128)(2,1)}, u32[]{:S(2)}) copy-start(bf16[4096,128]{1,0:T(8,128)(2,1)} %copy-done.4) | copy-start | bytes 3145732
  431.3 15.8 %copy-start.25 = (bf16[4096,128]{1,0:T(8,128)(2,1)S(1)}, bf16[4096,128]{1,0:T(8,128)(2,1)}, u32[]{:S(2)}) copy-start(bf16[4096,128]{1,0:T(8,128)(2,1)} %copy-done.24) | copy-start | bytes 3145732
  432.4 15.8 %copy-start.23 = (bf16[4096,128]{1,0:T(8,128)(2,1)S(1)}, bf16[4096,128]{1,0:T(8,128)(2,1)}, u32[]{:S(2)}) copy-start(bf16[4096,128]{1,0:T(8,128)(2,1)} %copy-done.22) | copy-start | bytes 3145732
  433.5 15.8 %copy-start.21 = (bf16[4096,128]{1,0:T(8,128)(2,1)S(1)}, bf16[4096,128]{1,0:T(8,128)(2,1)}, u32[]{:S(2)}) copy-start(bf16[4096,128]{1,0:T(8,128)(2,1)} %copy-done.20) | copy-start | bytes 3145732
  434.6 15.8 %copy-start.19 = (bf16[4096,128]{1,0:T(8,128)(2,1)S(1)}, bf16[4096,128]{1,0:T(8,128)(2,1)}, u32[]{:S(2)}) copy-start(bf16[4096,128]{1,0:T(8,128)(2,1)} %copy-done.18) | copy-start | bytes 3145732
  505.3 59.2 %copy-start.29 = (f32[2048]{0:T(1024)S(1)}, f32[2048]{0:T(1024)}, u32[]{:S(2)}) copy-start(f32[2048]{0:T(1024)} %param.19) | copy-start | bytes 24580
  556.5 8.0 %copy-start.1 = (f32[512,2048]{1,0:T(8,128)S(1)}, f32[512,2048]{1,0:T(8,128)}, u32[]{:S(2)}) copy-start(f32[512,2048]{1,0:T(8,128)} %copy-done) | copy-start | bytes 12582916
  556.5 8.0 %copy-start.2 = (bf16[512,2048]{1,0:T(8,128)(2,1)S(1)}, bf16[512,2048]{1,0:T(8,128)(2,1)}, u32[]{:S(2)}) copy-start(bf16[512,2048]{1,0:T(8,128)(2,1)} %reduce-scatter.2.cloned.1.call-done) | copy-start | bytes 6291460
Sparse Core Ops, SparseCore 0:
  76.9 59.4 all-gather.2
  138.6 154.6 all-gather.4
  505.5 50.9 reduce-scatter.1
